TPU v7x, 32 devices: a whole 2x2x4 slice. The times are simulated.
32 devices in a mesh: kv: 8 (over z, y), tp: 4 (over x, core).
Axes of the slice: x: 2, y: 2, z: 4, core: 2. Of those that a mesh axis runs over, the one named last changes fastest.
Arguments:
- tokens: bfloat16 [16, 4096], P(None, ('kv', 'tp')), may hold values from -6 to 6
- gain_attn: bfloat16 [4096], replicated, may hold values from 0.099609375 to 1.8984375
- w_query: bfloat16 [4096, 2048], P('kv', 'tp'), may hold values from -0.09375 to 0.09375
- w_key: bfloat16 [4096, 2048], P('kv', 'tp'), may hold values from -0.09375 to 0.09375
- w_value: bfloat16 [4096, 2048], P('kv', 'tp'), may hold values from -0.09375 to 0.09375
- w_forget: bfloat16 [4096, 32], replicated, may hold values from -0.09375 to 0.09375
- forget_bias: float32 [32], replicated, may hold values from -2 to 2
- keys_cache: bfloat16 [16, 4096, 2048], P(None, 'kv', 'tp'), may hold values from -900 to 900
- values_cache: bfloat16 [16, 4096, 2048], P(None, 'kv', 'tp'), may hold values from -6 to 6
- gates_cache: float32 [16, 32, 4096], P(None, 'tp', 'kv'), as said below
- lengths: int32 [16], replicated, may hold values from 1 to 4096, 32768 in all
- w_out: bfloat16 [2048, 4096], P('tp', 'kv'), may hold values from -0.1875 to 0.1875
- gain_mixer: bfloat16 [4096], replicated, may hold values from 0.099609375 to 1.8984375
- w_up: bfloat16 [4096, 16384], P('kv', 'tp'), may hold values from -0.09375 to 0.09375
- w_down: bfloat16 [16384, 4096], P('tp', 'kv'), may hold values from -0.0625 to 0.0625
Outputs:
- output: bfloat16 [16, 4096], P(None, ('kv', 'tp'))
Inputs may be any that keep to these rules, and one draw needn't show every extreme that they name: One sequence has all 4096 positions live; the lengths add up to half of 16 times 4096. `gates_cache`: along positions each entry is the running sum of per-position log forget gates up to and including that position, so the values never rise.
All inputs are finite; a program needn't handle non-finite values.
Results may differ from a plain program's by a relative error of at most 0.017.
Values may be sent and summed in bfloat16 or wider, within the bound.
No kernel may reach another device: no remote copies, remote signals or barrier semaphores. Data moves between devices by JAX's collectives and lax.ppermute only.
A program may use at most 128 MiB of HBM per device.

v0:
```python
import jax
import jax.numpy as jnp
from jax import lax
from jax.sharding import PartitionSpec as P

norm_eps = 1e-06


def combined_all(value, axis, join):
    pieces = jax.tree.map(lambda part: lax.all_gather(part, axis), value)
    head = jax.tree.map(lambda part: part[0], pieces)
    tail = jax.tree.map(lambda part: part[1:], pieces)
    total, _ = lax.scan(lambda total, section: (join(total, section), None), head, tail)
    return total


def combine_parts(earlier, later):
    top = jnp.maximum(earlier[0], later[0])
    early_factor = jnp.exp(earlier[0] - top)
    late_factor = jnp.exp(later[0] - top)
    totals = earlier[1] * early_factor + later[1] * late_factor
    summed = earlier[2] * early_factor[..., None] + later[2] * late_factor[..., None]
    return (top, totals, summed, earlier[3] + later[3])


def channel_mix(residual, gain_mixer, w_up, w_down, kv_index):
    width = gain_mixer.shape[0]
    block_start = kv_index * w_up.shape[0]
    piece = lax.all_gather(residual, "tp", axis=1, tiled=True)
    piece_f = piece.astype(jnp.float32)
    gain_part = lax.dynamic_slice_in_dim(gain_mixer, block_start, piece.shape[1], 0).astype(
        jnp.float32
    )
    scaled = (piece_f * gain_part).astype(jnp.bfloat16)
    upward = jnp.dot(scaled, w_up, preferred_element_type=jnp.float32)
    upward, squares = (upward, jnp.sum(piece_f * piece_f, axis=-1))
    up_total, square_total = lax.psum((upward, squares), "kv")
    mixer_scale = lax.rsqrt(square_total / width + norm_eps)
    active = jax.nn.relu(mixer_scale[:, None] * up_total)
    hidden = (active * active).astype(jnp.bfloat16)
    down = jnp.dot(hidden, w_down, preferred_element_type=jnp.float32)
    return lax.psum_scatter(down, "tp", scatter_dimension=1, tiled=True)


def shards(
    tokens,
    gain_attn,
    w_query,
    w_key,
    w_value,
    w_forget,
    forget_bias,
    keys_cache,
    values_cache,
    gates_cache,
    lengths,
    w_out,
    gain_mixer,
    w_up,
    w_down,
):
    kv_index = lax.axis_index("kv")
    tp_index = lax.axis_index("tp")
    row_block = w_query.shape[0]
    heads_here = gates_cache.shape[1]
    width = gain_attn.shape[0]
    row_start = kv_index * row_block
    head_start = tp_index * heads_here
    block_raw = lax.all_gather(tokens, "tp", axis=1, tiled=True)
    block_f = block_raw.astype(jnp.float32)
    gain_block = lax.dynamic_slice_in_dim(gain_attn, row_start, row_block, 0).astype(jnp.float32)
    block = (block_f * gain_block).astype(jnp.bfloat16)
    forget_block = lax.dynamic_slice(w_forget, (row_start, head_start), (row_block, heads_here))
    part_query = jnp.dot(block, w_query, preferred_element_type=jnp.float32)
    part_key = jnp.dot(block, w_key, preferred_element_type=jnp.float32)
    part_value = jnp.dot(block, w_value, preferred_element_type=jnp.float32)
    part_gate = jnp.dot(block, forget_block, preferred_element_type=jnp.float32)
    part_squares = jnp.sum(block_f * block_f, axis=-1)
    sum_query, sum_key, sum_value, sum_gate, squares = lax.psum(
        (part_query, part_key, part_value, part_gate, part_squares), "kv"
    )
    attn_scale = lax.rsqrt(squares / width + norm_eps)[:, None]
    gate_logit = attn_scale * sum_gate
    query = (attn_scale * sum_query).astype(jnp.bfloat16)
    new_key = (attn_scale * sum_key).astype(jnp.bfloat16)
    new_value = (attn_scale * sum_value).astype(jnp.bfloat16)
    bias_here = lax.dynamic_slice_in_dim(forget_bias, head_start, heads_here, 0)
    forget_log = jax.nn.log_sigmoid(gate_logit + bias_here)
    seqs = tokens.shape[0]
    positions_here = keys_cache.shape[1]
    query_heads = query.reshape(seqs, heads_here, -1)
    head_size = query_heads.shape[-1]
    keys_heads = keys_cache.reshape(seqs, positions_here, heads_here, head_size)
    values_heads = values_cache.reshape(seqs, positions_here, heads_here, head_size)
    scores = jnp.einsum(
        "bhd,bphd->bhp", query_heads, keys_heads, preferred_element_type=jnp.float32
    )
    logits = scores * head_size ** (-0.5) - gates_cache
    positions = kv_index * positions_here + jnp.arange(positions_here, dtype=jnp.int32)
    valid = (positions[None, :] < lengths[:, None])[:, None, :]
    local_top = jnp.max(jnp.where(valid, logits, -1e30), axis=-1)
    weights = jnp.where(valid, jnp.exp(logits - local_top[..., None]), 0.0)
    local_total = jnp.sum(weights, axis=-1)
    local_sum = jnp.einsum(
        "bhp,bphd->bhd",
        weights.astype(jnp.bfloat16),
        values_heads,
        preferred_element_type=jnp.float32,
    )
    at_last = (positions[None, :] == lengths[:, None] - 1)[:, None, :]
    last_local = jnp.sum(jnp.where(at_last, gates_cache, 0.0), axis=-1)
    top, totals, summed, last_gate = combined_all(
        (local_top, local_total, local_sum, last_local), "kv", combine_parts
    )
    top = top + last_gate + forget_log
    own = jnp.sum(
        query_heads.astype(jnp.float32) * new_key.reshape(seqs, heads_here, -1).astype(jnp.float32),
        axis=-1,
    ) * head_size ** (-0.5)
    overall = jnp.maximum(top, own)
    cache_factor = jnp.exp(top - overall)
    own_weight = jnp.exp(own - overall)
    denominator = totals * cache_factor + own_weight
    numerator = summed * cache_factor[..., None] + own_weight[..., None] * new_value.reshape(
        seqs, heads_here, -1
    ).astype(jnp.float32)
    mixed = (numerator / denominator[..., None]).astype(jnp.bfloat16).reshape(seqs, -1)
    partial_value = jnp.dot(mixed, w_out, preferred_element_type=jnp.float32).astype(jnp.bfloat16)
    attended = lax.psum_scatter(partial_value, "tp", scatter_dimension=1, tiled=True).astype(
        jnp.float32
    )
    residual = (tokens.astype(jnp.float32) + attended).astype(jnp.bfloat16)
    mixer = channel_mix(residual, gain_mixer, w_up, w_down, kv_index)
    return (residual.astype(jnp.float32) + mixer).astype(jnp.bfloat16)


def solution(mesh):
    return jax.shard_map(
        shards,
        mesh=mesh,
        in_specs=(
            P(None, ("kv", "tp")),
            P(),
            P("kv", "tp"),
            P("kv", "tp"),
            P("kv", "tp"),
            P(),
            P(),
            P(None, "kv", "tp"),
            P(None, "kv", "tp"),
            P(None, "tp", "kv"),
            P(),
            P("tp", "kv"),
            P(),
            P("kv", "tp"),
            P("tp", "kv"),
        ),
        out_specs=P(None, ("kv", "tp")),
        check_vma=False,
    )
```

profile of v0, /device:TPU:0, one launch (start us, length us, event | category | flops | bytes accessed | tf_op | source)
XLA Modules:
  0.0 361.5 jit_solution(17292253141642095304)
XLA Ops:
  6.5 6.5 %all_gather.30 = bf16[16,512]{1,0:T(8,128)(2,1)S(1)} all-gather(bf16[16,128]{1,0:T(8,128)(2,1)} %param.17), channel_id=1, replica_groups=mesh['kv'=8,'tp'=4] {'tp'}, dimensions={1}, use_global_device_ids=true | all-gather | bytes 20480 | tf_op jit(solution)/shard_map/all_gather | solution.py:69
  13.0 0.6 fusion.12
  13.7 0.8 dynamic-slice_convert_fusion.1
  14.4 0.8 fusion.25
  15.2 1.8 fusion.28
  17.1 1.8 fusion.23
  18.9 1.4 fusion.21
  20.4 0.7 broadcast_add_fusion
  21.0 0.7 broadcast_compare_fusion
  21.8 12.3 %copy.32 = bf16[16,512,512]{1,2,0:T(8,128)(2,1)} copy(bf16[16,512,512]{2,1,0:T(8,128)(2,1)} %param.24) | data formatting | bytes 16777216 | tf_op args[7]
  34.1 12.3 %copy.35 = bf16[16,512,512]{1,2,0:T(8,128)(2,1)} copy(bf16[16,512,512]{2,1,0:T(8,128)(2,1)} %param.25) | data formatting | bytes 16777216 | tf_op args[8]
  46.5 46.6 %all-reduce.6.cloned.1.call-done = (f32[16,512]{1,0:T(8,128)}, f32[16]{0:T(128)}, f32[16,512]{1,0:T(8,128)}, f32[16,8]{0,1:T(8,128)}, f32[16,512]{1,0:T(8,128)}) async-done(((f32[16,512]{1,0:T(8,128)}, f32[16]{0:T(128)}, f32[16,512]{1,0:T(8,128)}, f32[16,8]{0,1:T(8,128)}, f32[16,512]{1,0:T(8,128)}), (f32[16,512]{1,0:T(8,128)}, f32[16]{0:T(128)}, f32[16,512]{1,0:T(8,128)}, f32[16,8]{0,1:T(8,128)}, ...) | async-done | bytes 98896 | tf_op jit(solution)/shard_map/psum | solution.py:79
  93.1 0.7 add_rsqrt_fusion.1
  93.8 0.9 fusion.16
  94.6 0.1 reshape.122
  94.8 4.7 %fusion.38 = f32[16,8,1,512]{3,2,1,0:T(1,128)S(1)} fusion(bf16[16,8,64,1]{2,3,1,0:T(2,128)(2,1)S(1)} %reshape.122, bf16[16,512,8,64]{1,3,2,0:T(8,128)(2,1)} %bitcast.59), kind=kOutput, calls=%fused_computation.68 | convolution fusion | flops 8388608 | bytes 8667136 | tf_op jit(solution)/shard_map/bhd,bphd->bhp/dot_general | solution.py:95
  99.5 0.1 select_reduce_fusion.1
  99.6 0.2 select_reduce_fusion
  99.8 0.7 slice-done.1
  100.6 2.3 fusion.4
  102.8 31.3 %all-gather.2 = f32[128,8,64]{2,1,0:T(8,128)S(1)} all-gather(f32[16,8,64]{2,1,0:T(8,128)S(1)} %bitcast.65), channel_id=4, replica_groups=mesh['kv'=8,'tp'=4] {'kv'}, dimensions={0}, use_global_device_ids=true | all-gather | bytes 294912 | tf_op jit(solution)/shard_map/all_gather | solution.py:10
  134.2 30.6 %all-gather.6 = f32[8,16,8]{1,2,0:T(8,128)S(1)} all-gather(f32[1,16,8]{1,2,0:T(8,128)S(1)} %bitcast.67), channel_id=5, replica_groups=mesh['kv'=8,'tp'=4] {'kv'}, dimensions={0}, use_global_device_ids=true | all-gather | bytes 4608 | tf_op jit(solution)/shard_map/all_gather | solution.py:10
  164.9 30.6 %all-gather.5 = f32[8,16,8]{1,2,0:T(8,128)S(1)} all-gather(f32[1,16,8]{1,2,0:T(8,128)S(1)} %bitcast.68), channel_id=3, replica_groups=mesh['kv'=8,'tp'=4] {'kv'}, dimensions={0}, use_global_device_ids=true | all-gather | bytes 4608 | tf_op jit(solution)/shard_map/all_gather | solution.py:10
  195.6 30.6 %all-gather.4 = f32[8,16,8]{1,2,0:T(8,128)S(1)} all-gather(f32[1,16,8]{1,2,0:T(8,128)S(1)} %bitcast.69), channel_id=2, replica_groups=mesh['kv'=8,'tp'=4] {'kv'}, dimensions={0}, use_global_device_ids=true | all-gather | bytes 4608 | tf_op jit(solution)/shard_map/all_gather | solution.py:10
  226.2 0.1 reshape.80
  226.3 2.1 while.16
  226.5 0.1 fusion.52
  226.8 0.1 fusion.52
  227.1 0.1 fusion.52
  227.4 0.1 fusion.52
  227.7 0.1 fusion.52
  228.0 0.1 fusion.52
  228.3 0.1 fusion.52
  229.1 0.1 divide_convert_fusion
  229.2 0.1 reshape.83
  229.3 0.2 convolution_convert_fusion
  229.5 0.8 copy.45
  230.3 0.8 dynamic-slice_convert_fusion
  231.1 19.4 %reduce-scatter.7.cloned.1.call-done = bf16[128,16]{1,0:T(8,128)(2,1)} async-done(((bf16[512,16]{1,0:T(8,128)(2,1)}), bf16[128,16]{1,0:T(8,128)(2,1)}) %reduce-scatter.7.cloned.1.call-update) | async-done | bytes 4112
  250.5 0.8 copy.46
  251.3 5.2 %all_gather.39 = bf16[16,512]{1,0:T(8,128)(2,1)S(1)} all-gather(bf16[16,128]{1,0:T(8,128)(2,1)S(1)} %add_convert_fusion.1), channel_id=1, replica_groups=mesh['kv'=8,'tp'=4] {'tp'}, dimensions={1}, use_global_device_ids=true | all-gather | bytes 20480 | tf_op jit(solution)/shard_map/all_gather | solution.py:29
  256.5 3.5 fusion.18
  260.1 0.1 fusion.14
  260.2 21.4 %psum.54 = f32[16]{0:T(128)S(1)} all-reduce(f32[16]{0:T(128)S(1)} %fusion.14), channel_id=1, replica_groups=mesh['kv'=8,'tp'=4] {'kv'}, use_global_device_ids=true, to_apply=%region_14.15 | all-reduce | flops 16 | bytes 128 | tf_op jit(solution)/shard_map/psum | solution.py:37
  281.6 49.6 %all-reduce.4.cloned.1.call-done = f32[16,4096]{1,0:T(8,128)} async-done(((f32[16,4096]{1,0:T(8,128)}), f32[16,4096]{1,0:T(8,128)}) %all-reduce.4.cloned.1.call-update) | async-done | bytes 262160 | tf_op jit(solution)/shard_map/psum | solution.py:37
  331.2 3.6 fusion.9
  334.8 18.9 %reduce-scatter.5.cloned.1.call-done = f32[16,128]{1,0:T(8,128)} async-done(((f32[16,512]{1,0:T(8,128)}), f32[16,128]{1,0:T(8,128)}) %reduce-scatter.5.cloned.1.call-update) | async-done | bytes 8208 | tf_op jit(solution)/shard_map/reduce_scatter | solution.py:42
  353.7 1.3 add_convert_fusion
  (68 shorter events, 2.3 us)
Async XLA Ops:
  6.5 7.9 %copy-start = (bf16[512,512]{1,0:T(8,128)(2,1)S(1)}, bf16[512,512]{1,0:T(8,128)(2,1)}, u32[]{:S(2)}) copy-start(bf16[512,512]{1,0:T(8,128)(2,1)} %param.20) | copy-start | bytes 1572868
  6.5 86.6 %all-reduce.6.cloned.1.call-start = ((), (), s32[]{:S(2)}) async-start(), calls=%async_computation.5 | async-start | bytes 205824 | tf_op jit(solution)/shard_map/psum | solution.py:79
  20.3 230.1 %reduce-scatter.7.cloned.1.call-start = ((), (), s32[]{:S(2)}) async-start(), calls=%async_computation.4 | async-start | bytes 163840
  34.1 12.3 %copy-start.5 = (f32[32]{0:T(128)S(1)}, f32[32]{0:T(128)}, u32[]{:S(2)}) copy-start(f32[32]{0:T(128)} %param.23) | copy-start | bytes 388
  46.4 53.1 %copy-start.1 = (f32[16,8,512]{2,1,0:T(8,128)S(1)}, f32[16,8,512]{2,1,0:T(8,128)}, u32[]{:S(2)}) copy-start(f32[16,8,512]{2,1,0:T(8,128)} %param.26) | copy-start | bytes 786436
  94.7 5.1 %slice-start = ((s8[8388608]{0:T(1024)(128)(4,1)}), s8[4194304]{0:T(1024)(128)(4,1)S(1)}, s32[]{:S(2)}) async-start(s8[8388608]{0:T(1024)(128)(4,1)} %bitcast.60), calls=%async_computation.6 | async-start | bytes 8388608
  94.7 5.8 %slice-start.1 = ((s8[8388608]{0:T(1024)(128)(4,1)}), s8[4194304]{0:T(1024)(128)(4,1)S(1)}, s32[]{:S(2)}) async-start(s8[8388608]{0:T(1024)(128)(4,1)} %bitcast.60), calls=%async_computation.7 | async-start | bytes 8388608
  99.5 129.2 %copy-start.4 = (f32[16,8]{0,1:T(8,128)S(1)}, f32[16,8]{0,1:T(8,128)}, u32[]{:S(2)}) copy-start(f32[16,8]{0,1:T(8,128)} %get-tuple-element.82) | copy-start | bytes 1540
  99.5 129.8 %copy-start.2 = (bf16[512,512]{1,0:T(8,128)(2,1)S(1)}, bf16[512,512]{1,0:T(8,128)(2,1)}, u32[]{:S(2)}) copy-start(bf16[512,512]{1,0:T(8,128)(2,1)} %param.28) | copy-start | bytes 1572868
  99.5 151.8 %copy-start.3 = (bf16[16,128]{1,0:T(8,128)(2,1)S(1)}, bf16[16,128]{1,0:T(8,128)(2,1)}, u32[]{:S(2)}) copy-start(bf16[16,128]{1,0:T(8,128)(2,1)} %param.17) | copy-start | bytes 12292
  230.2 101.0 %all-reduce.4.cloned.1.call-start = ((), (), s32[]{:S(2)}) async-start(), calls=%async_computation.2 | async-start | bytes 524288 | tf_op jit(solution)/shard_map/psum | solution.py:37
  260.1 93.7 %reduce-scatter.5.cloned.1.call-start = ((), (), s32[]{:S(2)}) async-start(), calls=%async_computation.3 | async-start | bytes 40960 | tf_op jit(solution)/shard_map/reduce_scatter | solution.py:42
Sparse Core Ops, SparseCore 0:
  20.4 72.6 all-reduce.5
  230.4 20.0 reduce-scatter.6
  260.2 71.0 all-reduce.3
  335.0 18.6 reduce-scatter.4
where the time goes:
time: 363 us; the launch traced here: 362 us
  blocking collectives  156 us (43%)
  waiting for transfers between devices  135 us (37%)
  local copies, waits for them, and re-layouts  29.1 us (8%)
  matrix products  20.1 us (6%)
  between operations  13.3 us (4%)
  other arithmetic  8.07 us (2%)
    all_gather x4, blocking collectives, combined_all(): pieces = jax.tree.map(lambda part: lax.all_gather(part, axis), value)  123 us
    psum x1, waiting for transfers between devices, channel_mix(): up_total, square_total = lax.psum((upward, squares), 'kv')  49.6 us
    psum x1, waiting for transfers between devices, shards(): lax.psum((part_query, part_key, part_value, part_gate, part_squares), 'kv')  46.6 us
    unnamed x20, local copies, waits for them, and re-layouts  27 us
    psum x1, blocking collectives, channel_mix(): up_total, square_total = lax.psum((upward, squares), 'kv')  21.4 us
    unnamed x5, waiting for transfers between devices  19.5 us
    reduce_scatter x1, waiting for transfers between devices, channel_mix(): return lax.psum_scatter(down, 'tp', scatter_dimension=1, tiled=True)  18.9 us
  transfers between devices with their start and end apart: 4, of which 4 were waited for; matrix products, arithmetic and copies ran while one was open for 7% of the time, Pallas kernels for 0%

commit v1 on v0

v1 whole, which is shorter than its diff:
```python
import functools

import jax
import jax.numpy as jnp
from jax import lax
from jax.experimental import pallas as pl
from jax.experimental.pallas import tpu as pltpu
from jax.sharding import PartitionSpec as P

norm_eps = 1e-06
f32 = jnp.float32
bf16 = jnp.bfloat16
lanes = 128


def padded(width):
    return -(-width // lanes) * lanes


def exchange(pieces, axis):
    return lax.all_to_all(pieces, axis, 0, 0)


def broadcast(piece, axis):
    return exchange(jnp.broadcast_to(piece[None], (lax.axis_size(axis),) + piece.shape), axis)


def split3(value):
    high = value.astype(bf16)
    rest = value - high.astype(f32)
    middle = rest.astype(bf16)
    return high, middle, (rest - middle.astype(f32)).astype(bf16)


def head_mask(heads, width):
    row = lax.broadcasted_iota(jnp.int32, (heads, width), 0)
    column = lax.broadcasted_iota(jnp.int32, (heads, width), 1)
    size = width // heads
    return (column >= row * size) & (column < (row + 1) * size)


def project_kernel(block_ref, gain_ref, wq_ref, wk_ref, wv_ref, wf_ref, out_ref):
    raw = block_ref[...].astype(f32)
    block = (raw * gain_ref[...].astype(f32)).astype(bf16)
    count = out_ref.shape[0]
    gates = jnp.dot(block, wf_ref[...], preferred_element_type=f32)
    squares = jnp.sum(raw * raw, axis=-1, keepdims=True)
    piece = wq_ref.shape[1] // count
    for slot, ref in enumerate((wq_ref, wk_ref, wv_ref)):
        part = jnp.dot(block, ref[...], preferred_element_type=f32)
        for d in range(count):
            out_ref[d, :, slot * piece : (slot + 1) * piece] = part[:, d * piece : (d + 1) * piece]
    heads = gates.shape[1]
    for d in range(count):
        out_ref[d, :, 3 * piece : 3 * piece + heads] = gates
        out_ref[d, :, 3 * piece + heads : 3 * piece + heads + 1] = squares


def attend_kernel(info_ref, qkv_ref, keys_ref, values_ref, gates_ref, out_ref, query_ref):
    seq = pl.program_id(0)
    count = qkv_ref.shape[0]
    piece = qkv_ref.shape[2] // 3
    heads, positions = gates_ref.shape[1], gates_ref.shape[2]
    width = keys_ref.shape[2]
    size = width // heads

    @pl.when(seq == 0)
    def _():
        for d in range(count):
            query_ref[:, d * piece : (d + 1) * piece] = qkv_ref[d, :, :piece].astype(f32)
        out_ref[...] = jnp.zeros(out_ref.shape, f32)

    mask = head_mask(heads, width)
    here = lax.broadcasted_iota(jnp.int32, query_ref.shape, 0) == seq
    query = jnp.sum(jnp.where(here, query_ref[...], 0.0), axis=0, keepdims=True)
    query = jnp.where(mask, query, 0.0).astype(bf16)
    scores = lax.dot_general(
        query, keys_ref[0], (((1,), (1,)), ((), ())), preferred_element_type=f32
    )
    gates = gates_ref[0]
    logits = scores * size ** (-0.5) - gates
    live = info_ref[seq] - info_ref[info_ref.shape[0] - 1] * positions
    where = lax.broadcasted_iota(jnp.int32, (heads, positions), 1)
    valid = where < live
    top = jnp.max(jnp.where(valid, logits, -1e30), axis=-1, keepdims=True)
    weights = jnp.where(valid, jnp.exp(logits - top), 0.0)
    total = jnp.sum(weights, axis=-1, keepdims=True)
    last = jnp.sum(jnp.where(where == live - 1, gates, 0.0), axis=-1, keepdims=True)
    summed = jnp.dot(weights.astype(bf16), values_ref[0], preferred_element_type=f32)
    summed = jnp.sum(jnp.where(mask, summed, 0.0), axis=0, keepdims=True)
    out_ref[:, :width] = jnp.where(here, summed, out_ref[:, :width])
    extra = out_ref.shape[1] - width
    row = lax.broadcasted_iota(jnp.int32, (heads, extra), 0)
    column = lax.broadcasted_iota(jnp.int32, (heads, extra), 1)
    stats = jnp.where(column == row, top, 0.0)
    stats = stats + jnp.where(column == row + heads, total, 0.0)
    stats = stats + jnp.where(column == row + 2 * heads, last, 0.0)
    stats = jnp.sum(stats, axis=0, keepdims=True)
    out_ref[:, width:] = jnp.where(here[:, :extra], stats, out_ref[:, width:])


def combine_kernel(parts_ref, qkv_ref, forget_ref, w_ref, out_ref):
    count = parts_ref.shape[0]
    seqs, heads = forget_ref.shape
    width = w_ref.shape[0]
    piece = qkv_ref.shape[2] // 3
    size = width // heads
    spread = head_mask(heads, width).astype(f32)

    def joined(slot):
        return jnp.concatenate(
            [
                qkv_ref[d, :, slot * piece : (slot + 1) * piece].astype(f32)
                for d in range(count)
            ],
            axis=1,
        )

    query, key, value = joined(0), joined(1), joined(2)
    own = lax.dot_general(
        query * key,
        spread,
        (((1,), (1,)), ((), ())),
        precision=lax.Precision.HIGHEST,
        preferred_element_type=f32,
    ) * size ** (-0.5)
    tops = [parts_ref[d, :, width : width + heads] for d in range(count)]
    peak = functools.reduce(jnp.maximum, tops)
    last = sum(parts_ref[d, :, width + 2 * heads : width + 3 * heads] for d in range(count))
    top = peak + last + forget_ref[...]
    overall = jnp.maximum(top, own)
    shared = jnp.exp(top - overall)
    own_weight = jnp.exp(own - overall)
    factors = [jnp.exp(t - peak) * shared for t in tops]
    total = own_weight
    for d in range(count):
        total = total + parts_ref[d, :, width + heads : width + 2 * heads] * factors[d]
    inverse = 1.0 / total
    small = jnp.concatenate([f * inverse for f in factors] + [own_weight * inverse], axis=0)
    wide = jnp.dot(small, spread, precision=lax.Precision.HIGHEST, preferred_element_type=f32)
    mixed = wide[count * seqs :] * value
    for d in range(count):
        mixed = mixed + wide[d * seqs : (d + 1) * seqs] * parts_ref[d, :, :width]
    out_ref[...] = jnp.dot(
        mixed.astype(bf16), w_ref[...], preferred_element_type=f32
    ).astype(bf16)


def up_kernel(tokens_ref, parts_ref, gain_ref, w_ref, out_ref, residual_ref, scaled_ref, squares_ref):
    @pl.when(pl.program_id(0) == 0)
    def _():
        attended = sum(parts_ref[t].astype(f32) for t in range(parts_ref.shape[0]))
        residual = (tokens_ref[...].astype(f32) + attended).astype(bf16)
        residual_ref[...] = residual
        wide = residual.astype(f32)
        scaled_ref[...] = (wide * gain_ref[...].astype(f32)).astype(bf16)
        squares_ref[...] = jnp.broadcast_to(
            jnp.sum(wide * wide, axis=-1, keepdims=True), squares_ref.shape
        )

    count = out_ref.shape[0]
    piece = w_ref.shape[1] // count
    up = jnp.dot(scaled_ref[...], w_ref[...], preferred_element_type=f32).astype(bf16)
    extra = out_ref.shape[2] - piece
    column = lax.broadcasted_iota(jnp.int32, (up.shape[0], extra), 1)
    squares = squares_ref[:, :1]
    high, middle, low = (part.astype(f32) for part in split3(squares))
    tail = jnp.where(column == 0, high, jnp.where(column == 1, middle, low)).astype(bf16)
    for d in range(count):
        out_ref[d, :, :piece] = up[:, d * piece : (d + 1) * piece]
        out_ref[d, :, piece:] = tail


def down_kernel(hidden_ref, w_ref, out_ref, total_ref):
    step = pl.program_id(0)
    count = hidden_ref.shape[0]
    hidden = jnp.concatenate([hidden_ref[d] for d in range(count)], axis=1)
    down = jnp.dot(hidden, w_ref[...], preferred_element_type=f32)

    @pl.when(step == 0)
    def _():
        total_ref[...] = down

    @pl.when(step > 0)
    def _():
        total_ref[...] += down

    @pl.when(step == pl.num_programs(0) - 1)
    def _():
        groups = out_ref.shape[0]
        part = out_ref.shape[2]
        for t in range(groups):
            out_ref[t] = total_ref[:, t * part : (t + 1) * part]


def shards(
    tokens,
    gain_attn,
    w_query,
    w_key,
    w_value,
    w_forget,
    forget_bias,
    keys_cache,
    values_cache,
    gates_cache,
    lengths,
    w_out,
    gain_mixer,
    w_up,
    w_down,
):
    kv_index = lax.axis_index("kv")
    tp_index = lax.axis_index("tp")
    kv_count = lax.axis_size("kv")
    tp_count = lax.axis_size("tp")
    rows, width = w_query.shape
    seqs, heads, positions = gates_cache.shape
    features = gain_attn.shape[0]
    all_heads = w_forget.shape[1]
    piece = width // kv_count
    row_start = kv_index * rows

    block = lax.all_gather(tokens, "tp", axis=1, tiled=True)
    gain_block = lax.dynamic_slice_in_dim(gain_attn, row_start, rows, 0)[None]
    forget_block = lax.dynamic_slice_in_dim(w_forget, row_start, rows, 0)
    parts = pl.pallas_call(
        project_kernel,
        name="project",
        out_shape=jax.ShapeDtypeStruct((kv_count, seqs, 3 * piece + all_heads + 1), f32),
    )(block, gain_block, w_query, w_key, w_value, forget_block)
    sums = jnp.sum(exchange(parts, "kv"), axis=0)
    scale = lax.rsqrt(sums[:, -1:] / features + norm_eps)
    qkv = broadcast((scale * sums[:, : 3 * piece]).astype(bf16), "kv")
    bias = lax.dynamic_slice_in_dim(forget_bias, tp_index * heads, heads, 0)
    gate_sums = lax.dynamic_slice_in_dim(
        sums[:, 3 * piece : -1], tp_index * heads, heads, 1
    )
    forget_log = jax.nn.log_sigmoid(scale * gate_sums + bias)

    info = jnp.concatenate([lengths, kv_index[None].astype(jnp.int32)])
    wide = width + padded(3 * heads)
    local = pl.pallas_call(
        attend_kernel,
        name="attend",
        grid_spec=pltpu.PrefetchScalarGridSpec(
            num_scalar_prefetch=1,
            grid=(seqs,),
            in_specs=[
                pl.BlockSpec(qkv.shape, lambda b, info: (0, 0, 0)),
                pl.BlockSpec((1, positions, width), lambda b, info: (b, 0, 0)),
                pl.BlockSpec((1, positions, width), lambda b, info: (b, 0, 0)),
                pl.BlockSpec((1, heads, positions), lambda b, info: (b, 0, 0)),
            ],
            out_specs=pl.BlockSpec((seqs, wide), lambda b, info: (0, 0)),
            scratch_shapes=[pltpu.VMEM((seqs, width), f32)],
        ),
        out_shape=jax.ShapeDtypeStruct((seqs, wide), f32),
    )(info, qkv, keys_cache, values_cache, gates_cache)
    gathered = broadcast(local, "kv")
    head_part = pl.pallas_call(
        combine_kernel,
        name="combine",
        out_shape=jax.ShapeDtypeStruct((seqs, w_out.shape[1]), bf16),
    )(gathered, qkv, forget_log, w_out)
    head_parts = lax.all_gather(head_part, "tp")

    hidden_piece = w_up.shape[1] // kv_count
    together = max(1, min(kv_count, 512 // hidden_piece))
    steps = kv_count // together
    up_wide = hidden_piece + padded(hidden_piece + 3) - hidden_piece
    gain_part = lax.dynamic_slice_in_dim(gain_mixer, row_start, rows, 0)[None]
    ups, residual = pl.pallas_call(
        up_kernel,
        name="up",
        grid=(steps,),
        in_specs=[
            pl.BlockSpec(block.shape, lambda s: (0, 0)),
            pl.BlockSpec(head_parts.shape, lambda s: (0, 0, 0)),
            pl.BlockSpec(gain_part.shape, lambda s: (0, 0)),
            pl.BlockSpec((rows, together * hidden_piece), lambda s: (0, s)),
        ],
        out_specs=[
            pl.BlockSpec((together, seqs, up_wide), lambda s: (s, 0, 0)),
            pl.BlockSpec(block.shape, lambda s: (0, 0)),
        ],
        scratch_shapes=[pltpu.VMEM(block.shape, bf16), pltpu.VMEM((seqs, lanes), f32)],
        out_shape=[
            jax.ShapeDtypeStruct((kv_count, seqs, up_wide), bf16),
            jax.ShapeDtypeStruct(block.shape, bf16),
        ],
    )(block, head_parts, gain_part, w_up)
    up_sums = jnp.sum(exchange(ups, "kv").astype(f32), axis=0)
    squares = up_sums[:, hidden_piece : hidden_piece + 3].sum(axis=-1, keepdims=True)
    mixer_scale = lax.rsqrt(squares / features + norm_eps)
    active = jax.nn.relu(mixer_scale * up_sums[:, :hidden_piece])
    hidden = broadcast((active * active).astype(bf16), "kv")
    out_width = w_down.shape[1]
    downs = pl.pallas_call(
        down_kernel,
        name="down",
        grid=(steps,),
        in_specs=[
            pl.BlockSpec((together, seqs, hidden_piece), lambda s: (s, 0, 0)),
            pl.BlockSpec((together * hidden_piece, out_width), lambda s: (s, 0)),
        ],
        out_specs=pl.BlockSpec((tp_count, seqs, out_width // tp_count), lambda s: (0, 0, 0)),
        scratch_shapes=[pltpu.VMEM((seqs, out_width), f32)],
        out_shape=jax.ShapeDtypeStruct((tp_count, seqs, out_width // tp_count), f32),
    )(hidden, w_down)
    mixer = jnp.sum(exchange(downs, "tp"), axis=0)
    mine = lax.dynamic_slice_in_dim(residual, tp_index * mixer.shape[1], mixer.shape[1], 1)
    return (mine.astype(f32) + mixer).astype(bf16)


def solution(mesh):
    return jax.shard_map(
        shards,
        mesh=mesh,
        in_specs=(
            P(None, ("kv", "tp")),
            P(),
            P("kv", "tp"),
            P("kv", "tp"),
            P("kv", "tp"),
            P(),
            P(),
            P(None, "kv", "tp"),
            P(None, "kv", "tp"),
            P(None, "tp", "kv"),
            P(),
            P("tp", "kv"),
            P(),
            P("kv", "tp"),
            P("tp", "kv"),
        ),
        out_specs=P(None, ("kv", "tp")),
        check_vma=False,
    )
```

time: 363 us -> 122 us (0.34)
  waiting for transfers between devices: 135 us -> 15.9 us
  blocking collectives: 156 us -> 49.2 us
  Pallas kernels: 0 us -> 33.6 us
  local copies, waits for them, and re-layouts: 29.1 us -> 8.02 us
  matrix products: 20.1 us -> 0 us
  between operations: 13.3 us -> 0.07 us
  starting transfers between devices: 0.13 us -> 10 us
  other arithmetic: 8.07 us -> 3.71 us
    all_gather x6 -> x2, blocking collectives: 135 us -> 13.9 us  [the longest x1 8.02 us: shards(): block = lax.all_gather(tokens, 'tp', axis=1, tiled=True)]
    psum x2 -> x0, waiting for transfers between devices: 96.2 us -> none  [the longest x1 49.6 us: channel_mix(): up_total, square_total = lax.psum((upward, squares), 'kv')]
    all_to_all x0 -> x3, blocking collectives: none -> 35.3 us  [exchange(): return lax.all_to_all(pieces, axis, 0, 0)]
    pallas_call x0 -> x5, Pallas kernels: none -> 33.6 us  [the longest x1 16.1 us: shards(): pl.pallas_call(attend_kernel, name='attend', grid_spec=pltpu.PrefetchScal...]
    unnamed x20 -> x9, local copies, waits for them, and re-layouts: 27 us -> 3.03 us
    psum x1 -> x0, blocking collectives: 21.4 us -> none  [channel_mix(): up_total, square_total = lax.psum((upward, squares), 'kv')]
    dot_general x9 -> x0, matrix products: 20.1 us -> none  [the longest x1 4.72 us: shards(): jnp.einsum('bhd,bphd->bhp', query_heads, keys_heads, preferred_element_ty...]
    unnamed x5 -> x0, waiting for transfers between devices: 19.5 us -> none
  transfers between devices with their start and end apart: 4 -> 3, of which waited for: 4 -> 3; matrix products, arithmetic and copies ran while one was open for 7% -> 3% of each run, Pallas kernels for 0% -> 0%
where the time goes in v1:
time: 122 us; the launch traced here: 121 us
  blocking collectives  49.2 us (40%)
  Pallas kernels  33.6 us (28%)
  waiting for transfers between devices  15.9 us (13%)
  starting transfers between devices  10 us (8%)
  local copies, waits for them, and re-layouts  8.02 us (7%)
  other arithmetic  3.71 us (3%)
    all_to_all x3, blocking collectives, exchange(): return lax.all_to_all(pieces, axis, 0, 0)  35.3 us
    pallas_call x1, Pallas kernels, shards(): pl.pallas_call(attend_kernel, name='attend', grid_spec=pltpu.PrefetchScal...  16.1 us
    all_to_all x3, waiting for transfers between devices, exchange(): return lax.all_to_all(pieces, axis, 0, 0)  15.9 us
    all_to_all x3, starting transfers between devices, exchange(): return lax.all_to_all(pieces, axis, 0, 0)  10 us
    all_gather x1, blocking collectives, shards(): block = lax.all_gather(tokens, 'tp', axis=1, tiled=True)  8.02 us
    pallas_call x1, Pallas kernels, shards(): pl.pallas_call(up_kernel, name='up', grid=(steps,), in_specs=[pl.BlockSpe...  6.33 us
    all_gather x1, blocking collectives, shards(): head_parts = lax.all_gather(head_part, 'tp')  5.93 us
    pallas_call x1, Pallas kernels, shards(): pl.pallas_call(down_kernel, name='down', grid=(steps,), in_specs=[pl.Bloc...  5.89 us
  transfers between devices with their start and end apart: 3, of which 3 were waited for; matrix products, arithmetic and copies ran while one was open for 3% of the time, Pallas kernels for 0%

profile of v1, /device:TPU:0, one launch (start us, length us, event | category | flops | bytes accessed | tf_op | source)
XLA Modules:
  0.0 120.6 jit_solution(7023759535396773395)
XLA Ops:
  0.0 0.0 copy-start
  0.0 0.9 copy-done
  1.0 0.7 copy.18.wf_ref
  1.7 0.8 dynamic_slice.18
  2.5 0.6 broadcast_in_dim.13.gain_ref
  3.0 8.0 %all_gather.9.block_ref.tokens_ref = bf16[16,512]{1,0:T(8,128)(2,1)} all-gather(bf16[16,128]{1,0:T(8,128)(2,1)} %param.15), channel_id=1, replica_groups=mesh['kv'=8,'tp'=4] {'tp'}, dimensions={1}, use_global_device_ids=true | all-gather | bytes 20480 | tf_op jit(solution)/shard_map/all_gather | solution.py:224
  11.1 2.5 %project.1 = f32[8,16,225]{2,1,0:T(8,128)} custom-call(bf16[16,512]{1,0:T(8,128)(2,1)} %all_gather.9.block_ref.tokens_ref, bf16[1,512]{1,0:T(2,128)(2,1)} %broadcast_in_dim.13.gain_ref, bf16[512,512]{1,0:T(8,128)(2,1)} %wq_ref.1, bf16[512,512]{1,0:T(8,128)(2,1)} %wk_ref.1, bf16[512,512]{1,0:T(8,128)(2,1)} %wv_ref.1, bf16[512,32]{1,0:T(8,128)(2,1)} %copy.18.wf_ref), custom_call_target="tpu_custom_call" | custom-call | tf_op jit(solution)/shard_map/project/pallas_call | solution.py:227
  13.5 13.3 %all_to_all.30 = f32[8,16,225]{2,1,0:T(8,128)S(1)} all-to-all(f32[8,16,225]{2,1,0:T(8,128)} %project.1), channel_id=1, replica_groups=mesh['kv'=8,'tp'=4] {'kv'}, dimensions={0} | all-to-all | bytes 230400 | tf_op jit(solution)/shard_map/all_to_all | solution.py:21
  26.9 0.2 fusion.7
  27.1 0.1 fusion.3
  27.1 0.6 broadcast_in_dim.14
  27.8 3.3 %all-to-all-start.1 = ((bf16[8,16,192]{2,1,0:T(8,128)(2,1)}), bf16[8,16,192]{2,1,0:T(8,128)(2,1)S(1)}, u32[]{:S(2)}, u32[]{:S(2)}) async-start(bf16[8,16,192]{2,1,0:T(8,128)(2,1)} %broadcast_in_dim.14), calls=%async_computation.1 | async-start | bytes 131072 | tf_op jit(solution)/shard_map/all_to_all | solution.py:21
  31.1 1.2 %pad_add_fusion.info_ref = s32[17]{0:T(128)} fusion(s32[1]{0:T(128)} %bitcast, s32[16]{0:T(128)} %param.25), kind=kLoop, calls=%fused_computation.16 | loop fusion | flops 17 | bytes 136 | tf_op jit(solution)/shard_map/concatenate | solution.py:241
  32.4 0.0 copy-start.3
  32.4 5.6 %all-to-all-done.1.qkv_ref = bf16[8,16,192]{2,1,0:T(8,128)(2,1)S(1)} async-done(((bf16[8,16,192]{2,1,0:T(8,128)(2,1)}), bf16[8,16,192]{2,1,0:T(8,128)(2,1)S(1)}, u32[]{:S(2)}, u32[]{:S(2)}) %all-to-all-start.1) | async-done | bytes 49184 | tf_op jit(solution)/shard_map/all_to_all | solution.py:21
  38.0 0.0 copy-start.2
  38.0 0.6 copy-done.2
  38.6 16.1 %attend.1 = f32[16,640]{1,0:T(8,128)} custom-call(s32[17]{0:T(128)} %pad_add_fusion.info_ref, bf16[8,16,192]{2,1,0:T(8,128)(2,1)} %copy-done.2, bf16[16,512,512]{2,1,0:T(8,128)(2,1)} %keys_ref.1, bf16[16,512,512]{2,1,0:T(8,128)(2,1)} %values_ref.1, f32[16,8,512]{2,1,0:T(8,128)} %gates_ref.1), custom_call_target="tpu_custom_call" | custom-call | tf_op jit(solution)/shard_map/attend/pallas_call | solution.py:243
  54.7 1.5 %broadcast_in_dim.15 = f32[8,16,640]{2,1,0:T(8,128)} broadcast(f32[16,640]{1,0:T(8,128)} %attend.1), dimensions={1,2} | broadcast | bytes 368640 | tf_op jit(solution)/shard_map/broadcast_in_dim | solution.py:25
  56.2 3.4 %all-to-all-start.2 = ((f32[8,16,640]{2,1,0:T(8,128)}), f32[8,16,640]{2,1,0:T(8,128)S(1)}, u32[]{:S(2)}, u32[]{:S(2)}) async-start(f32[8,16,640]{2,1,0:T(8,128)} %broadcast_in_dim.15), calls=%async_computation.2 | async-start | bytes 655360 | tf_op jit(solution)/shard_map/all_to_all | solution.py:21
  59.7 0.8 dynamic_slice.22
  60.4 0.6 broadcast_in_dim.16.gain_ref
  61.0 0.0 copy-done.3
  61.0 0.1 dynamic_slice.21
  61.1 0.1 slice.22
  61.2 0.7 fusion.4.forget_ref
  61.9 6.4 %all-to-all-done.2.parts_ref = f32[8,16,640]{2,1,0:T(8,128)S(1)} async-done(((f32[8,16,640]{2,1,0:T(8,128)}), f32[8,16,640]{2,1,0:T(8,128)S(1)}, u32[]{:S(2)}, u32[]{:S(2)}) %all-to-all-start.2) | async-done | bytes 327712 | tf_op jit(solution)/shard_map/all_to_all | solution.py:21
  68.3 0.0 copy-start.1
  68.3 0.7 copy-done.1
  69.0 2.8 %combine.1 = bf16[16,512]{1,0:T(8,128)(2,1)} custom-call(f32[8,16,640]{2,1,0:T(8,128)} %copy-done.1, bf16[8,16,192]{2,1,0:T(8,128)(2,1)} %copy-done.2, f32[16,8]{1,0:T(8,128)} %fusion.4.forget_ref, bf16[512,512]{1,0:T(8,128)(2,1)} %w_ref.3), custom_call_target="tpu_custom_call" | custom-call | tf_op jit(solution)/shard_map/combine/pallas_call | solution.py:261
  71.8 5.9 %all-gather = bf16[64,512]{1,0:T(8,128)(2,1)} all-gather(bf16[16,512]{1,0:T(8,128)(2,1)} %combine.1), channel_id=2, replica_groups=mesh['kv'=8,'tp'=4] {'tp'}, dimensions={0}, use_global_device_ids=true | all-gather | bytes 81920 | tf_op jit(solution)/shard_map/all_gather | solution.py:266
  77.7 6.3 %up.1 = (bf16[8,16,640]{2,1,0:T(8,128)(2,1)}, bf16[16,512]{1,0:T(8,128)(2,1)}) custom-call(bf16[16,512]{1,0:T(8,128)(2,1)} %all_gather.9.block_ref.tokens_ref, bf16[4,16,512]{2,1,0:T(8,128)(2,1)} %bitcast.2, bf16[1,512]{1,0:T(2,128)(2,1)} %broadcast_in_dim.16.gain_ref, bf16[512,4096]{1,0:T(8,128)(2,1)} %w_ref.4), custom_call_target="tpu_custom_call" | custom-call | tf_op jit(solution)/shard_map/up/pallas_call | solution.py:273
  84.0 11.5 %all_to_all.31 = bf16[8,16,640]{2,1,0:T(8,128)(2,1)S(1)} all-to-all(bf16[8,16,640]{2,1,0:T(8,128)(2,1)} %get-tuple-element.8), channel_id=1, replica_groups=mesh['kv'=8,'tp'=4] {'kv'}, dimensions={0} | all-to-all | bytes 327680 | tf_op jit(solution)/shard_map/all_to_all | solution.py:21
  95.6 0.1 slice_reduce_fusion
  95.7 0.1 fusion.2
  95.8 10.4 %all_to_all.32.hidden_ref = bf16[8,16,512]{2,1,0:T(8,128)(2,1)} all-to-all(bf16[8,16,512]{2,1,0:T(8,128)(2,1)S(1)} %broadcast_in_dim.34), channel_id=1, replica_groups=mesh['kv'=8,'tp'=4] {'kv'}, dimensions={0} | all-to-all | bytes 262144 | tf_op jit(solution)/shard_map/all_to_all | solution.py:21
  106.2 5.9 %down.1 = f32[4,16,128]{2,1,0:T(8,128)} custom-call(bf16[8,16,512]{2,1,0:T(8,128)(2,1)} %all_to_all.32.hidden_ref, bf16[4096,512]{1,0:T(8,128)(2,1)} %w_ref.5), custom_call_target="tpu_custom_call" | custom-call | tf_op jit(solution)/shard_map/down/pallas_call | solution.py:299
  112.1 3.3 %all-to-all-start.5 = ((f32[4,16,128]{2,1,0:T(8,128)}), f32[4,16,128]{2,1,0:T(8,128)S(1)}, u32[]{:S(2)}, u32[]{:S(2)}) async-start(f32[4,16,128]{2,1,0:T(8,128)} %down.1), calls=%async_computation.5 | async-start | bytes 65536 | tf_op jit(solution)/shard_map/all_to_all | solution.py:21
  115.4 3.9 %all-to-all-done.5 = f32[4,16,128]{2,1,0:T(8,128)S(1)} async-done(((f32[4,16,128]{2,1,0:T(8,128)}), f32[4,16,128]{2,1,0:T(8,128)S(1)}, u32[]{:S(2)}, u32[]{:S(2)}) %all-to-all-start.5) | async-done | bytes 32800 | tf_op jit(solution)/shard_map/all_to_all | solution.py:21
  119.3 1.3 %add_convert_fusion = bf16[16,128]{1,0:T(8,128)(2,1)} fusion(f32[16,128]{1,0:T(8,128)S(1)} %reduce_sum.39, bf16[16,512]{1,0:T(8,128)(2,1)} %get-tuple-element.7, s32[]{:T(128)S(6)} %select_n.20), kind=kLoop, calls=%fused_computation.14 | loop fusion | flops 6144 | bytes 16388 | tf_op jit(solution)/shard_map/convert_element_type | solution.py:313
  (6 shorter events, 0.1 us)
Async XLA Ops:
  0.0 1.0 copy-start
  27.8 10.2 %all-to-all-start.1 = ((bf16[8,16,192]{2,1,0:T(8,128)(2,1)}), bf16[8,16,192]{2,1,0:T(8,128)(2,1)S(1)}, u32[]{:S(2)}, u32[]{:S(2)}) async-start(bf16[8,16,192]{2,1,0:T(8,128)(2,1)} %broadcast_in_dim.14), calls=%async_computation.1 | async-start | bytes 131072 | tf_op jit(solution)/shard_map/all_to_all | solution.py:21
  32.4 28.6 %copy-start.3 = (f32[32]{0:T(128)S(1)}, f32[32]{0:T(128)}, u32[]{:S(2)}) copy-start(f32[32]{0:T(128)} %param.21) | copy-start | bytes 388
  38.0 0.6 copy-start.2
  56.2 12.0 %all-to-all-start.2 = ((f32[8,16,640]{2,1,0:T(8,128)}), f32[8,16,640]{2,1,0:T(8,128)S(1)}, u32[]{:S(2)}, u32[]{:S(2)}) async-start(f32[8,16,640]{2,1,0:T(8,128)} %broadcast_in_dim.15), calls=%async_computation.2 | async-start | bytes 655360 | tf_op jit(solution)/shard_map/all_to_all | solution.py:21
  68.3 0.7 copy-start.1
  112.1 7.2 %all-to-all-start.5 = ((f32[4,16,128]{2,1,0:T(8,128)}), f32[4,16,128]{2,1,0:T(8,128)S(1)}, u32[]{:S(2)}, u32[]{:S(2)}) async-start(f32[4,16,128]{2,1,0:T(8,128)} %down.1), calls=%async_computation.5 | async-start | bytes 65536 | tf_op jit(solution)/shard_map/all_to_all | solution.py:21

commit v2 on v1

v2 whole, which is shorter than its diff:
```python
import functools

import jax
import jax.numpy as jnp
from jax import lax
from jax.experimental import pallas as pl
from jax.experimental.pallas import tpu as pltpu
from jax.sharding import PartitionSpec as P

norm_eps = 1e-06
f32 = jnp.float32
bf16 = jnp.bfloat16
lanes = 128


def padded(width):
    return -(-width // lanes) * lanes


def exchange(pieces, axis):
    return lax.all_to_all(pieces, axis, 0, 0)


def broadcast(piece, axis):
    return exchange(jnp.broadcast_to(piece[None], (lax.axis_size(axis),) + piece.shape), axis)


def split3(value):
    high = value.astype(bf16)
    rest = value - high.astype(f32)
    middle = rest.astype(bf16)
    return high, middle, (rest - middle.astype(f32)).astype(bf16)


def head_mask(heads, width):
    row = lax.broadcasted_iota(jnp.int32, (heads, width), 0)
    column = lax.broadcasted_iota(jnp.int32, (heads, width), 1)
    size = width // heads
    return (column >= row * size) & (column < (row + 1) * size)


def project_kernel(
    info_ref, block_ref, gain_ref, wq_ref, wk_ref, wv_ref, wf_ref, out_ref, key_ref, value_ref
):
    raw = block_ref[...].astype(f32)
    block = (raw * gain_ref[...].astype(f32)).astype(bf16)
    width = wq_ref.shape[1]
    heads = wf_ref.shape[0]
    query = jnp.dot(block, wq_ref[...], preferred_element_type=f32)
    gates = lax.dot_general(
        block, wf_ref[...], (((1,), (1,)), ((), ())), preferred_element_type=f32
    )
    squares = jnp.sum(raw * raw, axis=-1, keepdims=True)
    for d in range(out_ref.shape[0]):
        out_ref[d, :, :width] = query
        out_ref[d, :, width : width + heads] = gates
        out_ref[d, :, width + heads : width + heads + 1] = squares
    key_ref[...] = jnp.dot(block, wk_ref[...], preferred_element_type=f32)
    value_ref[...] = jnp.dot(block, wv_ref[...], preferred_element_type=f32)


def attend_kernel(
    features,
    info_ref,
    parts_ref,
    key_ref,
    value_ref,
    bias_ref,
    keys_ref,
    values_ref,
    gates_ref,
    out_ref,
    forget_ref,
    sums_ref,
    stats_ref,
    keys_near,
    values_near,
    sems,
):
    count = parts_ref.shape[0]
    seqs, heads, positions = gates_ref.shape
    pairs = ((keys_ref, keys_near), (values_ref, values_near))
    copies = [
        [
            pltpu.make_async_copy(source.at[b], target.at[b], sems.at[i, b])
            for i, (source, target) in enumerate(pairs)
        ]
        for b in range(seqs)
    ]
    for both in copies:
        for copy in both:
            copy.start()
    width = keys_ref.shape[2]
    all_heads = bias_ref.shape[1]
    size = width // heads
    step = size ** (-0.5)
    mask = head_mask(heads, width)
    total_in = parts_ref[0]
    for d in range(1, count):
        total_in = total_in + parts_ref[d]
    scale = lax.rsqrt(total_in[:, width + all_heads : width + all_heads + 1] / features + norm_eps)
    query = (scale * total_in[:, :width]).astype(bf16)
    gate = scale * total_in[:, width : width + all_heads] + bias_ref[...]
    log_gate = jnp.minimum(gate, 0.0) - jnp.log1p(jnp.exp(-jnp.abs(gate)))
    row = lax.broadcasted_iota(jnp.int32, (all_heads, heads), 0)
    column = lax.broadcasted_iota(jnp.int32, (all_heads, heads), 1)
    pick = (row == column + info_ref[seqs + 1] * heads).astype(f32)
    forget_ref[...] = jnp.dot(
        log_gate, pick, precision=lax.Precision.HIGHEST, preferred_element_type=f32
    )
    wide = query.astype(f32)
    start = info_ref[seqs] * positions
    where = lax.broadcasted_iota(jnp.int32, (heads, positions), 1)
    lane_row = lax.broadcasted_iota(jnp.int32, (heads, lanes), 0)
    lane = lax.broadcasted_iota(jnp.int32, (heads, lanes), 1)
    for b in range(seqs):
        spread = jnp.where(mask, wide[b : b + 1], 0.0).astype(bf16)
        for copy in copies[b]:
            copy.wait()
        scores = lax.dot_general(
            spread, keys_near[b], (((1,), (1,)), ((), ())), preferred_element_type=f32
        )
        gates = gates_ref[b]
        logits = scores * step - gates
        live = info_ref[b] - start
        valid = where < live
        top = jnp.max(jnp.where(valid, logits, -1e30), axis=-1, keepdims=True)
        weights = jnp.where(valid, jnp.exp(logits - top), 0.0)
        total = jnp.sum(weights, axis=-1, keepdims=True)
        last = jnp.sum(jnp.where(where == live - 1, gates, 0.0), axis=-1, keepdims=True)
        summed = jnp.dot(weights.astype(bf16), values_near[b], preferred_element_type=f32)
        sums_ref[b : b + 1, :] = jnp.sum(jnp.where(mask, summed, 0.0), axis=0, keepdims=True)
        stats = jnp.where(lane == lane_row, top, 0.0)
        stats = jnp.where(lane == lane_row + heads, total, stats)
        stats = jnp.where(lane == lane_row + 2 * heads, last, stats)
        stats_ref[b : b + 1, :] = jnp.sum(stats, axis=0, keepdims=True)
    own = lax.dot_general(
        wide * key_ref[...],
        mask.astype(f32),
        (((1,), (1,)), ((), ())),
        precision=lax.Precision.HIGHEST,
        preferred_element_type=f32,
    ) * (scale * step)
    sums = sums_ref[...].astype(bf16)
    value = (scale * value_ref[...]).astype(bf16)
    tails = split3(stats_ref[:, : 3 * heads]) + split3(own)
    spots = [2 * width + 4 * heads * i for i in range(3)]
    spots = spots + [spot + 3 * heads for spot in spots]
    for d in range(count):
        out_ref[d, :, :width] = sums
        out_ref[d, :, width : 2 * width] = value
        for spot, tail in zip(spots, tails):
            out_ref[d, :, spot : spot + tail.shape[1]] = tail


def combine_kernel(parts_ref, forget_ref, w_ref, out_ref):
    count = parts_ref.shape[0]
    seqs, heads = forget_ref.shape
    width = w_ref.shape[0]
    spread = head_mask(heads, width).astype(f32)
    stats = []
    for d in range(count):
        tails = [
            parts_ref[d, :, 2 * width + 4 * heads * i : 2 * width + 4 * heads * (i + 1)].astype(f32)
            for i in range(3)
        ]
        stats.append(tails[0] + tails[1] + tails[2])
    tops = [part[:, :heads] for part in stats]
    peak = functools.reduce(jnp.maximum, tops)
    joint = functools.reduce(jnp.add, stats)
    own = joint[:, 3 * heads :]
    top = peak + joint[:, 2 * heads : 3 * heads] + forget_ref[...]
    overall = jnp.maximum(top, own)
    shared = jnp.exp(top - overall)
    own_weight = jnp.exp(own - overall)
    factors = [jnp.exp(t - peak) * shared for t in tops]
    total = own_weight
    for d in range(count):
        total = total + stats[d][:, heads : 2 * heads] * factors[d]
    inverse = 1.0 / total
    small = jnp.concatenate([f * inverse for f in factors] + [own_weight * inverse], axis=0)
    wide = jnp.dot(small, spread, precision=lax.Precision.HIGHEST, preferred_element_type=f32)
    value = parts_ref[0, :, width : 2 * width].astype(f32)
    for d in range(1, count):
        value = value + parts_ref[d, :, width : 2 * width].astype(f32)
    mixed = wide[count * seqs :] * value
    for d in range(count):
        mixed = mixed + wide[d * seqs : (d + 1) * seqs] * parts_ref[d, :, :width].astype(f32)
    out_ref[...] = jnp.dot(
        mixed.astype(bf16), w_ref[...], preferred_element_type=f32
    ).astype(bf16)


def started(sources, targets, sems):
    copies = [
        pltpu.make_async_copy(source, target, sems.at[i])
        for i, (source, target) in enumerate(zip(sources, targets))
    ]
    for copy in copies:
        copy.start()
    return copies


def up_kernel(
    together, tokens_ref, parts_ref, gain_ref, w_ref, out_ref, residual_ref, near_ref, sems
):
    count = out_ref.shape[0]
    block = w_ref.shape[1] // near_ref.shape[0]
    piece = w_ref.shape[1] // count
    steps = near_ref.shape[0]
    copies = started(
        [w_ref.at[:, s * block : (s + 1) * block] for s in range(steps)],
        [near_ref.at[s] for s in range(steps)],
        sems,
    )
    attended = sum(parts_ref[t].astype(f32) for t in range(parts_ref.shape[0]))
    residual = (tokens_ref[...].astype(f32) + attended).astype(bf16)
    residual_ref[...] = residual
    wide = residual.astype(f32)
    scaled = (wide * gain_ref[...].astype(f32)).astype(bf16)
    tails = split3(jnp.sum(wide * wide, axis=-1, keepdims=True))
    for s in range(steps):
        copies[s].wait()
        up = jnp.dot(scaled, near_ref[s], preferred_element_type=f32).astype(bf16)
        for d in range(together):
            out_ref[s * together + d, :, :piece] = up[:, d * piece : (d + 1) * piece]
            for i, tail in enumerate(tails):
                out_ref[s * together + d, :, piece + i : piece + i + 1] = tail


def down_kernel(together, hidden_ref, w_ref, out_ref, near_ref, sems):
    steps = near_ref.shape[0]
    block = near_ref.shape[1]
    copies = started(
        [w_ref.at[s * block : (s + 1) * block] for s in range(steps)],
        [near_ref.at[s] for s in range(steps)],
        sems,
    )
    down = 0.0
    for s in range(steps):
        hidden = jnp.concatenate(
            [hidden_ref[s * together + d] for d in range(together)], axis=1
        )
        copies[s].wait()
        down = down + jnp.dot(hidden, near_ref[s], preferred_element_type=f32)
    groups = out_ref.shape[0]
    part = out_ref.shape[2]
    for t in range(groups):
        out_ref[t] = down[:, t * part : (t + 1) * part]


def far(value):
    return pltpu.with_memory_space_constraint(value, pltpu.HBM)


in_vmem = pl.BlockSpec(memory_space=pltpu.VMEM)
in_hbm = pl.BlockSpec(memory_space=pltpu.HBM)
in_smem = pl.BlockSpec(memory_space=pltpu.SMEM)
small_limit = pltpu.CompilerParams(vmem_limit_bytes=16 * 2**20)


def shards(
    tokens,
    gain_attn,
    w_query,
    w_key,
    w_value,
    w_forget,
    forget_bias,
    keys_cache,
    values_cache,
    gates_cache,
    lengths,
    w_out,
    gain_mixer,
    w_up,
    w_down,
):
    kv_index = lax.axis_index("kv")
    tp_index = lax.axis_index("tp")
    kv_count = lax.axis_size("kv")
    tp_count = lax.axis_size("tp")
    rows, width = w_query.shape
    seqs, heads, positions = gates_cache.shape
    features = gain_attn.shape[0]
    all_heads = w_forget.shape[1]
    place = jnp.stack([kv_index, tp_index]).astype(jnp.int32)
    info = jnp.concatenate([lengths, place])

    block = lax.all_gather(tokens, "tp", axis=1, tiled=True)
    whole = pl.BlockSpec((rows, width), lambda s, at: (0, 0))
    small = pl.BlockSpec((seqs, width), lambda s, at: (0, 0))
    part_shape = (kv_count, seqs, width + padded(all_heads + 1))
    parts, part_key, part_value = pl.pallas_call(
        project_kernel,
        name="project",
        grid_spec=pltpu.PrefetchScalarGridSpec(
            num_scalar_prefetch=1,
            grid=(1,),
            in_specs=[
                pl.BlockSpec((seqs, rows), lambda s, at: (0, 0)),
                pl.BlockSpec((1, rows), lambda s, at: (0, at[0])),
                whole,
                whole,
                whole,
                pl.BlockSpec((all_heads, rows), lambda s, at: (0, at[0])),
            ],
            out_specs=[pl.BlockSpec(part_shape, lambda s, at: (0, 0, 0)), small, small],
        ),
        out_shape=[
            jax.ShapeDtypeStruct(part_shape, f32),
            jax.ShapeDtypeStruct((seqs, width), f32),
            jax.ShapeDtypeStruct((seqs, width), f32),
        ],
        compiler_params=small_limit,
    )(place, block, gain_attn[None], far(w_query), far(w_key), far(w_value), far(w_forget.T))

    wide = 2 * width + padded(12 * heads)
    local, forget_log = pl.pallas_call(
        functools.partial(attend_kernel, features),
        name="attend",
        in_specs=[in_smem] + [in_vmem] * 4 + [in_hbm] * 2 + [in_vmem],
        scratch_shapes=[
            pltpu.VMEM((seqs, width), f32),
            pltpu.VMEM((seqs, lanes), f32),
            pltpu.VMEM(keys_cache.shape, bf16),
            pltpu.VMEM(values_cache.shape, bf16),
            pltpu.SemaphoreType.DMA((2, seqs)),
        ],
        out_shape=[
            jax.ShapeDtypeStruct((kv_count, seqs, wide), bf16),
            jax.ShapeDtypeStruct((seqs, heads), f32),
        ],
        compiler_params=pltpu.CompilerParams(vmem_limit_bytes=32 * 2**20),
    )(
        info,
        exchange(parts, "kv"),
        part_key,
        part_value,
        forget_bias[None],
        far(keys_cache),
        far(values_cache),
        gates_cache,
    )
    head_part = pl.pallas_call(
        combine_kernel,
        name="combine",
        in_specs=[in_vmem] * 3,
        out_shape=jax.ShapeDtypeStruct((seqs, w_out.shape[1]), bf16),
        compiler_params=small_limit,
    )(exchange(local, "kv"), forget_log, w_out)
    head_parts = lax.all_gather(head_part, "tp")

    hidden_piece = w_up.shape[1] // kv_count
    together = max(1, min(kv_count, 512 // hidden_piece))
    steps = kv_count // together
    up_wide = padded(hidden_piece + 3)
    gain_part = lax.dynamic_slice_in_dim(gain_mixer, kv_index * rows, rows, 0)[None]
    ups, residual = pl.pallas_call(
        functools.partial(up_kernel, together),
        name="up",
        in_specs=[in_vmem] * 3 + [in_hbm],
        scratch_shapes=[
            pltpu.VMEM((steps, rows, w_up.shape[1] // steps), bf16),
            pltpu.SemaphoreType.DMA((steps,)),
        ],
        out_shape=[
            jax.ShapeDtypeStruct((kv_count, seqs, up_wide), bf16),
            jax.ShapeDtypeStruct(block.shape, bf16),
        ],
        compiler_params=small_limit,
    )(block, head_parts, gain_part, far(w_up))
    up_sums = jnp.sum(exchange(ups, "kv").astype(f32), axis=0)
    squares = up_sums[:, hidden_piece : hidden_piece + 3].sum(axis=-1, keepdims=True)
    mixer_scale = lax.rsqrt(squares / features + norm_eps)
    active = jax.nn.relu(mixer_scale * up_sums[:, :hidden_piece])
    hidden = broadcast((active * active).astype(bf16), "kv")
    out_width = w_down.shape[1]
    downs = pl.pallas_call(
        functools.partial(down_kernel, together),
        name="down",
        in_specs=[in_vmem, in_hbm],
        scratch_shapes=[
            pltpu.VMEM((steps, w_down.shape[0] // steps, out_width), bf16),
            pltpu.SemaphoreType.DMA((steps,)),
        ],
        out_shape=jax.ShapeDtypeStruct((tp_count, seqs, out_width // tp_count), f32),
        compiler_params=small_limit,
    )(hidden, far(w_down))
    mixer = jnp.sum(exchange(downs, "tp"), axis=0)
    mine = lax.dynamic_slice_in_dim(residual, tp_index * mixer.shape[1], mixer.shape[1], 1)
    return (mine.astype(f32) + mixer).astype(bf16)


def solution(mesh):
    return jax.shard_map(
        shards,
        mesh=mesh,
        in_specs=(
            P(None, ("kv", "tp")),
            P(),
            P("kv", "tp"),
            P("kv", "tp"),
            P("kv", "tp"),
            P(),
            P(),
            P(None, "kv", "tp"),
            P(None, "kv", "tp"),
            P(None, "tp", "kv"),
            P(),
            P("tp", "kv"),
            P(),
            P("kv", "tp"),
            P("tp", "kv"),
        ),
        out_specs=P(None, ("kv", "tp")),
        check_vma=False,
    )
```

time: 122 us -> 95 us (0.78)
  blocking collectives: 49.2 us -> 33.1 us
  Pallas kernels: 33.6 us -> 20.3 us
  waiting for transfers between devices: 15.9 us -> 23 us
  local copies, waits for them, and re-layouts: 8.02 us -> 3.09 us
  starting transfers between devices: 10 us -> 13.2 us
  other arithmetic: 3.71 us -> 1.64 us
    all_to_all x3 -> x2, blocking collectives: 35.3 us -> 21.5 us  [exchange(): return lax.all_to_all(pieces, axis, 0, 0)]
    pallas_call x5, Pallas kernels: 33.6 us -> 20.3 us  [the longest x1 10.9 us: shards(): pl.pallas_call(functools.partial(attend_kernel, features), name='attend',...]
    all_to_all x3, waiting for transfers between devices: 15.9 us -> 23 us  [exchange(): return lax.all_to_all(pieces, axis, 0, 0)]
    all_to_all x3, starting transfers between devices: 10 us -> 13.2 us  [exchange(): return lax.all_to_all(pieces, axis, 0, 0)]
    broadcast_in_dim x3 -> x1, local copies, waits for them, and re-layouts: 2.16 us -> 0.01 us  [broadcast(): jnp.broadcast_to(piece[None], (lax.axis_size(axis),) + piece.shape)]
    all_gather x1, blocking collectives: 8.02 us -> 6.38 us  [shards(): block = lax.all_gather(tokens, 'tp', axis=1, tiled=True)]
    unnamed x9 -> x6, local copies, waits for them, and re-layouts: 3.03 us -> 1.61 us
  transfers between devices with their start and end apart: 3 -> 3, of which waited for: 3 -> 3; matrix products, arithmetic and copies ran while one was open for 3% -> 2% of each run, Pallas kernels for 0% -> 0%
where the time goes in v2:
time: 95 us; the launch traced here: 94.3 us
  blocking collectives  33.1 us (35%)
  waiting for transfers between devices  23 us (24%)
  Pallas kernels  20.3 us (21%)
  starting transfers between devices  13.2 us (14%)
  local copies, waits for them, and re-layouts  3.09 us (3%)
  other arithmetic  1.64 us (2%)
    all_to_all x3, waiting for transfers between devices, exchange(): return lax.all_to_all(pieces, axis, 0, 0)  23 us
    all_to_all x2, blocking collectives, exchange(): return lax.all_to_all(pieces, axis, 0, 0)  21.5 us
    all_to_all x3, starting transfers between devices, exchange(): return lax.all_to_all(pieces, axis, 0, 0)  13.2 us
    pallas_call x1, Pallas kernels, shards(): pl.pallas_call(functools.partial(attend_kernel, features), name='attend',...  10.9 us
    all_gather x1, blocking collectives, shards(): block = lax.all_gather(tokens, 'tp', axis=1, tiled=True)  6.38 us
    all_gather x1, blocking collectives, shards(): head_parts = lax.all_gather(head_part, 'tp')  5.24 us
    pallas_call x1, Pallas kernels, shards(): pl.pallas_call(functools.partial(down_kernel, together), name='down', in_...  3 us
    pallas_call x1, Pallas kernels, shards(): pl.pallas_call(project_kernel, name='project', grid_spec=pltpu.PrefetchSc...  2.83 us
  transfers between devices with their start and end apart: 3, of which 3 were waited for; matrix products, arithmetic and copies ran while one was open for 2% of the time, Pallas kernels for 0%

profile of v2, /device:TPU:0, one launch (start us, length us, event | category | flops | bytes accessed | tf_op | source)
XLA Modules:
  0.0 94.3 jit_solution(8721667159788876092)
XLA Ops:
  0.0 6.4 %all_gather.9.block_ref.tokens_ref = bf16[16,512]{1,0:T(8,128)(2,1)S(1)} all-gather(bf16[16,128]{1,0:T(8,128)(2,1)} %param.15), channel_id=1, replica_groups=mesh['kv'=8,'tp'=4] {'tp'}, dimensions={1}, use_global_device_ids=true | all-gather | bytes 20480 | tf_op jit(solution)/shard_map/all_gather | solution.py:290
  6.4 0.7 broadcast_in_dim.16.gain_ref
  7.1 0.1 pad_add_fusion.1.info_ref
  7.2 2.8 %project.1 = (f32[8,16,640]{2,1,0:T(8,128)}, f32[16,512]{1,0:T(8,128)S(1)}, f32[16,512]{1,0:T(8,128)S(1)}) custom-call(s32[2]{0:T(128)S(1)} %pad_add_fusion.1.info_ref, bf16[16,512]{1,0:T(8,128)(2,1)S(1)} %all_gather.9.block_ref.tokens_ref, bf16[1,4096]{1,0:T(2,128)(2,1)S(1)} %broadcast_in_dim.16.gain_ref, bf16[512,512]{1,0:T(8,128)(2,1)} %wq_ref.1, ...), custom_call_target="tpu_custom_call" | custom-call | tf_op jit(solution)/shard_map/project/pallas_call | solution.py:294
  10.0 6.3 %all-to-all-start = ((f32[8,16,640]{2,1,0:T(8,128)}), f32[8,16,640]{2,1,0:T(8,128)S(1)}, u32[]{:S(2)}, u32[]{:S(2)}) async-start(f32[8,16,640]{2,1,0:T(8,128)} %get-tuple-element.12), calls=%async_computation | async-start | bytes 655360 | tf_op jit(solution)/shard_map/all_to_all | solution.py:21
  16.3 0.7 pad_add_fusion.info_ref
  17.0 10.1 %all-to-all-done.parts_ref = f32[8,16,640]{2,1,0:T(8,128)S(1)} async-done(((f32[8,16,640]{2,1,0:T(8,128)}), f32[8,16,640]{2,1,0:T(8,128)S(1)}, u32[]{:S(2)}, u32[]{:S(2)}) %all-to-all-start) | async-done | bytes 327712 | tf_op jit(solution)/shard_map/all_to_all | solution.py:21
  27.1 0.0 copy-start.1
  27.1 0.9 %copy-done.1 = f32[16,8,512]{2,1,0:T(8,128)S(1)} copy-done((f32[16,8,512]{2,1,0:T(8,128)S(1)}, f32[16,8,512]{2,1,0:T(8,128)}, u32[]{:S(2)}) %copy-start.1) | copy-done | bytes 262168
  28.0 0.0 copy-start.2
  28.0 0.7 copy-done.2
  28.7 0.0 copy-start
  28.7 10.9 %attend.1 = (bf16[8,16,1152]{2,1,0:T(8,128)(2,1)}, f32[16,8]{1,0:T(8,128)S(1)}) custom-call(s32[18]{0:T(128)S(1)} %pad_add_fusion.info_ref, f32[8,16,640]{2,1,0:T(8,128)S(1)} %all-to-all-done.parts_ref, f32[16,512]{1,0:T(8,128)S(1)} %get-tuple-element.13.key_ref, f32[16,512]{1,0:T(8,128)S(1)} %get-tuple-element.14.value_ref, f32[1,32]{1,0:T(1,128)S(1)} %bitcast.6, ...), custom_call_target="tpu_custom_call" | custom-call | tf_op jit(solution)/shard_map/attend/pallas_call | solution.py:319
  39.6 3.6 %all-to-all-start.1 = ((bf16[8,16,1152]{2,1,0:T(8,128)(2,1)}), bf16[8,16,1152]{2,1,0:T(8,128)(2,1)S(1)}, u32[]{:S(2)}, u32[]{:S(2)}) async-start(bf16[8,16,1152]{2,1,0:T(8,128)(2,1)} %get-tuple-element.15), calls=%async_computation.1 | async-start | bytes 589824 | tf_op jit(solution)/shard_map/all_to_all | solution.py:21
  43.2 0.8 dynamic_slice.6
  44.0 9.0 %all-to-all-done.1.parts_ref = bf16[8,16,1152]{2,1,0:T(8,128)(2,1)S(1)} async-done(((bf16[8,16,1152]{2,1,0:T(8,128)(2,1)}), bf16[8,16,1152]{2,1,0:T(8,128)(2,1)S(1)}, u32[]{:S(2)}, u32[]{:S(2)}) %all-to-all-start.1) | async-done | bytes 294944 | tf_op jit(solution)/shard_map/all_to_all | solution.py:21
  53.0 0.0 copy-done
  53.0 0.9 combine.1
  53.9 5.2 %all-gather = bf16[64,512]{1,0:T(8,128)(2,1)S(1)} all-gather(bf16[16,512]{1,0:T(8,128)(2,1)S(1)} %combine.1), channel_id=2, replica_groups=mesh['kv'=8,'tp'=4] {'tp'}, dimensions={0}, use_global_device_ids=true | all-gather | bytes 81920 | tf_op jit(solution)/shard_map/all_gather | solution.py:352
  59.2 2.6 %up.1 = (bf16[8,16,640]{2,1,0:T(8,128)(2,1)S(1)}, bf16[16,512]{1,0:T(8,128)(2,1)S(1)}) custom-call(bf16[16,512]{1,0:T(8,128)(2,1)S(1)} %all_gather.9.block_ref.tokens_ref, bf16[4,16,512]{2,1,0:T(8,128)(2,1)S(1)} %bitcast.5, bf16[1,512]{1,0:T(2,128)(2,1)S(1)} %broadcast_in_dim.18.gain_ref, bf16[512,4096]{1,0:T(8,128)(2,1)} %w_ref.4), custom_call_target="tpu_custom_call" | custom-call | tf_op jit(solution)/shard_map/up/pallas_call | solution.py:359
  61.8 11.4 %all_to_all.25 = bf16[8,16,640]{2,1,0:T(8,128)(2,1)S(1)} all-to-all(bf16[8,16,640]{2,1,0:T(8,128)(2,1)S(1)} %get-tuple-element.18), channel_id=1, replica_groups=mesh['kv'=8,'tp'=4] {'kv'}, dimensions={0} | all-to-all | bytes 327680 | tf_op jit(solution)/shard_map/all_to_all | solution.py:21
  73.2 0.1 slice_reduce_fusion
  73.3 0.1 fusion.2
  73.5 10.1 %all_to_all.26.hidden_ref = bf16[8,16,512]{2,1,0:T(8,128)(2,1)S(1)} all-to-all(bf16[8,16,512]{2,1,0:T(8,128)(2,1)S(1)} %broadcast_in_dim.19), channel_id=1, replica_groups=mesh['kv'=8,'tp'=4] {'kv'}, dimensions={0} | all-to-all | bytes 262144 | tf_op jit(solution)/shard_map/all_to_all | solution.py:21
  83.5 3.0 %down.1 = f32[4,16,128]{2,1,0:T(8,128)} custom-call(bf16[8,16,512]{2,1,0:T(8,128)(2,1)S(1)} %all_to_all.26.hidden_ref, bf16[4096,512]{1,0:T(8,128)(2,1)} %w_ref.5), custom_call_target="tpu_custom_call" | custom-call | tf_op jit(solution)/shard_map/down/pallas_call | solution.py:379
  86.5 3.3 %all-to-all-start.4 = ((f32[4,16,128]{2,1,0:T(8,128)}), f32[4,16,128]{2,1,0:T(8,128)S(1)}, u32[]{:S(2)}, u32[]{:S(2)}) async-start(f32[4,16,128]{2,1,0:T(8,128)} %down.1), calls=%async_computation.4 | async-start | bytes 65536 | tf_op jit(solution)/shard_map/all_to_all | solution.py:21
  89.8 3.9 %all-to-all-done.4 = f32[4,16,128]{2,1,0:T(8,128)S(1)} async-done(((f32[4,16,128]{2,1,0:T(8,128)}), f32[4,16,128]{2,1,0:T(8,128)S(1)}, u32[]{:S(2)}, u32[]{:S(2)}) %all-to-all-start.4) | async-done | bytes 32800 | tf_op jit(solution)/shard_map/all_to_all | solution.py:21
  93.7 0.6 add_convert_fusion
  (5 shorter events, 0.1 us)
Async XLA Ops:
  10.0 17.1 %all-to-all-start = ((f32[8,16,640]{2,1,0:T(8,128)}), f32[8,16,640]{2,1,0:T(8,128)S(1)}, u32[]{:S(2)}, u32[]{:S(2)}) async-start(f32[8,16,640]{2,1,0:T(8,128)} %get-tuple-element.12), calls=%async_computation | async-start | bytes 655360 | tf_op jit(solution)/shard_map/all_to_all | solution.py:21
  27.1 1.0 %copy-start.1 = (f32[16,8,512]{2,1,0:T(8,128)S(1)}, f32[16,8,512]{2,1,0:T(8,128)}, u32[]{:S(2)}) copy-start(f32[16,8,512]{2,1,0:T(8,128)} %gates_ref.1) | copy-start | bytes 786436
  28.0 0.7 copy-start.2
  28.7 24.3 %copy-start = (bf16[512,512]{1,0:T(8,128)(2,1)S(1)}, bf16[512,512]{1,0:T(8,128)(2,1)}, u32[]{:S(2)}) copy-start(bf16[512,512]{1,0:T(8,128)(2,1)} %w_ref.3) | copy-start | bytes 1572868
  39.6 13.4 %all-to-all-start.1 = ((bf16[8,16,1152]{2,1,0:T(8,128)(2,1)}), bf16[8,16,1152]{2,1,0:T(8,128)(2,1)S(1)}, u32[]{:S(2)}, u32[]{:S(2)}) async-start(bf16[8,16,1152]{2,1,0:T(8,128)(2,1)} %get-tuple-element.15), calls=%async_computation.1 | async-start | bytes 589824 | tf_op jit(solution)/shard_map/all_to_all | solution.py:21
  86.5 7.2 %all-to-all-start.4 = ((f32[4,16,128]{2,1,0:T(8,128)}), f32[4,16,128]{2,1,0:T(8,128)S(1)}, u32[]{:S(2)}, u32[]{:S(2)}) async-start(f32[4,16,128]{2,1,0:T(8,128)} %down.1), calls=%async_computation.4 | async-start | bytes 65536 | tf_op jit(solution)/shard_map/all_to_all | solution.py:21

commit v3 on v2

--- a/solution.py
+++ b/solution.py
@@ -57,6 +57,16 @@
         out_ref[d, :, width + heads : width + heads + 1] = squares
     key_ref[...] = jnp.dot(block, wk_ref[...], preferred_element_type=f32)
     value_ref[...] = jnp.dot(block, wv_ref[...], preferred_element_type=f32)
+
+
+def started(sources, targets, sems):
+    copies = [
+        pltpu.make_async_copy(source, target, sems.at[i])
+        for i, (source, target) in enumerate(zip(sources, targets))
+    ]
+    for copy in copies:
+        copy.start()
+    return copies
 
 
 def attend_kernel(
@@ -75,10 +85,14 @@
     stats_ref,
     keys_near,
     values_near,
+    gates_near,
+    bias_near,
     sems,
+    side_sems,
 ):
     count = parts_ref.shape[0]
     seqs, heads, positions = gates_ref.shape
+    side = started([bias_ref, gates_ref], [bias_near, gates_near], side_sems)
     pairs = ((keys_ref, keys_near), (values_ref, values_near))
     copies = [
         [
@@ -100,7 +114,8 @@
         total_in = total_in + parts_ref[d]
     scale = lax.rsqrt(total_in[:, width + all_heads : width + all_heads + 1] / features + norm_eps)
     query = (scale * total_in[:, :width]).astype(bf16)
-    gate = scale * total_in[:, width : width + all_heads] + bias_ref[...]
+    side[0].wait()
+    gate = scale * total_in[:, width : width + all_heads] + bias_near[...]
     log_gate = jnp.minimum(gate, 0.0) - jnp.log1p(jnp.exp(-jnp.abs(gate)))
     row = lax.broadcasted_iota(jnp.int32, (all_heads, heads), 0)
     column = lax.broadcasted_iota(jnp.int32, (all_heads, heads), 1)
@@ -109,6 +124,7 @@
         log_gate, pick, precision=lax.Precision.HIGHEST, preferred_element_type=f32
     )
     wide = query.astype(f32)
+    side[1].wait()
     start = info_ref[seqs] * positions
     where = lax.broadcasted_iota(jnp.int32, (heads, positions), 1)
     lane_row = lax.broadcasted_iota(jnp.int32, (heads, lanes), 0)
@@ -120,7 +136,7 @@
         scores = lax.dot_general(
             spread, keys_near[b], (((1,), (1,)), ((), ())), preferred_element_type=f32
         )
-        gates = gates_ref[b]
+        gates = gates_near[b]
         logits = scores * step - gates
         live = info_ref[b] - start
         valid = where < live
@@ -191,16 +207,6 @@
     ).astype(bf16)
 
 
-def started(sources, targets, sems):
-    copies = [
-        pltpu.make_async_copy(source, target, sems.at[i])
-        for i, (source, target) in enumerate(zip(sources, targets))
-    ]
-    for copy in copies:
-        copy.start()
-    return copies
-
-
 def up_kernel(
     together, tokens_ref, parts_ref, gain_ref, w_ref, out_ref, residual_ref, near_ref, sems
 ):
@@ -243,10 +249,7 @@
         )
         copies[s].wait()
         down = down + jnp.dot(hidden, near_ref[s], preferred_element_type=f32)
-    groups = out_ref.shape[0]
-    part = out_ref.shape[2]
-    for t in range(groups):
-        out_ref[t] = down[:, t * part : (t + 1) * part]
+    out_ref[...] = down
 
 
 def far(value):
@@ -319,13 +322,16 @@
     local, forget_log = pl.pallas_call(
         functools.partial(attend_kernel, features),
         name="attend",
-        in_specs=[in_smem] + [in_vmem] * 4 + [in_hbm] * 2 + [in_vmem],
+        in_specs=[in_smem] + [in_vmem] * 3 + [in_hbm] * 4,
         scratch_shapes=[
             pltpu.VMEM((seqs, width), f32),
             pltpu.VMEM((seqs, lanes), f32),
             pltpu.VMEM(keys_cache.shape, bf16),
             pltpu.VMEM(values_cache.shape, bf16),
+            pltpu.VMEM(gates_cache.shape, f32),
+            pltpu.VMEM((1, all_heads), f32),
             pltpu.SemaphoreType.DMA((2, seqs)),
+            pltpu.SemaphoreType.DMA((2,)),
         ],
         out_shape=[
             jax.ShapeDtypeStruct((kv_count, seqs, wide), bf16),
@@ -337,10 +343,10 @@
         exchange(parts, "kv"),
         part_key,
         part_value,
-        forget_bias[None],
+        far(forget_bias[None]),
         far(keys_cache),
         far(values_cache),
-        gates_cache,
+        far(gates_cache),
     )
     head_part = pl.pallas_call(
         combine_kernel,
@@ -384,11 +390,13 @@
             pltpu.VMEM((steps, w_down.shape[0] // steps, out_width), bf16),
             pltpu.SemaphoreType.DMA((steps,)),
         ],
-        out_shape=jax.ShapeDtypeStruct((tp_count, seqs, out_width // tp_count), f32),
+        out_shape=jax.ShapeDtypeStruct((seqs, out_width), f32),
         compiler_params=small_limit,
     )(hidden, far(w_down))
-    mixer = jnp.sum(exchange(downs, "tp"), axis=0)
-    mine = lax.dynamic_slice_in_dim(residual, tp_index * mixer.shape[1], mixer.shape[1], 1)
+    gathered = lax.all_gather(downs, "tp")
+    share = out_width // tp_count
+    mixer = jnp.sum(lax.dynamic_slice_in_dim(gathered, tp_index * share, share, 2), axis=0)
+    mine = lax.dynamic_slice_in_dim(residual, tp_index * share, share, 1)
     return (mine.astype(f32) + mixer).astype(bf16)
 
 

time: 95 us -> 96.6 us (1.017)
  blocking collectives: 33.1 us -> 28.4 us
  Pallas kernels: 20.3 us -> 24.1 us
  waiting for transfers between devices: 23 us -> 26.3 us
    all_to_all x2 -> x1, blocking collectives: 21.5 us -> 11.4 us  [exchange(): return lax.all_to_all(pieces, axis, 0, 0)]
    all_gather x0 -> x1, blocking collectives: none -> 5.42 us  [shards(): gathered = lax.all_gather(downs, 'tp')]
    pallas_call x1, Pallas kernels: 10.9 us -> 15.4 us  [shards(): pl.pallas_call(functools.partial(attend_kernel, features), name='attend',...]
    all_to_all x3, waiting for transfers between devices: 23 us -> 26.3 us  [exchange(): return lax.all_to_all(pieces, axis, 0, 0)]
    unnamed x6 -> x2, local copies, waits for them, and re-layouts: 1.61 us -> 0.01 us
where the time goes in v3:
time: 96.6 us; the launch traced here: 96 us
  blocking collectives  28.4 us (29%)
  waiting for transfers between devices  26.3 us (27%)
  Pallas kernels  24.1 us (25%)
  starting transfers between devices  13.3 us (14%)
  local copies, waits for them, and re-layouts  2.13 us (2%)
  other arithmetic  1.64 us (2%)
    all_to_all x3, waiting for transfers between devices, exchange(): return lax.all_to_all(pieces, axis, 0, 0)  26.3 us
    pallas_call x1, Pallas kernels, shards(): pl.pallas_call(functools.partial(attend_kernel, features), name='attend',...  15.4 us
    all_to_all x3, starting transfers between devices, exchange(): return lax.all_to_all(pieces, axis, 0, 0)  13.3 us
    all_to_all x1, blocking collectives, exchange(): return lax.all_to_all(pieces, axis, 0, 0)  11.4 us
    all_gather x1, blocking collectives, shards(): block = lax.all_gather(tokens, 'tp', axis=1, tiled=True)  6.38 us
    all_gather x1, blocking collectives, shards(): gathered = lax.all_gather(downs, 'tp')  5.42 us
    all_gather x1, blocking collectives, shards(): head_parts = lax.all_gather(head_part, 'tp')  5.24 us
    pallas_call x1, Pallas kernels, shards(): pl.pallas_call(project_kernel, name='project', grid_spec=pltpu.PrefetchSc...  2.83 us
  transfers between devices with their start and end apart: 3, of which 3 were waited for; matrix products, arithmetic and copies ran while one was open for 2% of the time, Pallas kernels for 0%

profile of v3, /device:TPU:0, one launch (start us, length us, event | category | flops | bytes accessed | tf_op | source)
XLA Modules:
  0.0 96.0 jit_solution(4489712223324464934)
XLA Ops:
  0.0 6.4 %all_gather.15.block_ref.tokens_ref = bf16[16,512]{1,0:T(8,128)(2,1)S(1)} all-gather(bf16[16,128]{1,0:T(8,128)(2,1)} %param.15), channel_id=1, replica_groups=mesh['kv'=8,'tp'=4] {'tp'}, dimensions={1}, use_global_device_ids=true | all-gather | bytes 20480 | tf_op jit(solution)/shard_map/all_gather | solution.py:293
  6.4 0.7 broadcast_in_dim.16.gain_ref
  7.1 0.1 pad_add_fusion.1.info_ref
  7.2 2.8 %project.1 = (f32[8,16,640]{2,1,0:T(8,128)}, f32[16,512]{1,0:T(8,128)S(1)}, f32[16,512]{1,0:T(8,128)S(1)}) custom-call(s32[2]{0:T(128)S(1)} %pad_add_fusion.1.info_ref, bf16[16,512]{1,0:T(8,128)(2,1)S(1)} %all_gather.15.block_ref.tokens_ref, bf16[1,4096]{1,0:T(2,128)(2,1)S(1)} %broadcast_in_dim.16.gain_ref, bf16[512,512]{1,0:T(8,128)(2,1)} %wq_ref.1, ...), custom_call_target="tpu_custom_call" | custom-call | tf_op jit(solution)/shard_map/project/pallas_call | solution.py:297
  10.0 6.3 %all-to-all-start = ((f32[8,16,640]{2,1,0:T(8,128)}), f32[8,16,640]{2,1,0:T(8,128)S(1)}, u32[]{:S(2)}, u32[]{:S(2)}) async-start(f32[8,16,640]{2,1,0:T(8,128)} %get-tuple-element.12), calls=%async_computation | async-start | bytes 655360 | tf_op jit(solution)/shard_map/all_to_all | solution.py:21
  16.3 0.7 pad_add_fusion.info_ref
  17.0 10.1 %all-to-all-done.parts_ref = f32[8,16,640]{2,1,0:T(8,128)S(1)} async-done(((f32[8,16,640]{2,1,0:T(8,128)}), f32[8,16,640]{2,1,0:T(8,128)S(1)}, u32[]{:S(2)}, u32[]{:S(2)}) %all-to-all-start) | async-done | bytes 327712 | tf_op jit(solution)/shard_map/all_to_all | solution.py:21
  27.1 0.0 copy-start
  27.1 15.4 %attend.1 = (bf16[8,16,1152]{2,1,0:T(8,128)(2,1)}, f32[16,8]{1,0:T(8,128)S(1)}) custom-call(s32[18]{0:T(128)S(1)} %pad_add_fusion.info_ref, f32[8,16,640]{2,1,0:T(8,128)S(1)} %all-to-all-done.parts_ref, f32[16,512]{1,0:T(8,128)S(1)} %get-tuple-element.13.key_ref, f32[16,512]{1,0:T(8,128)S(1)} %get-tuple-element.14.value_ref, f32[1,32]{1,0:T(1,128)} %bitcast.9, ...), custom_call_target="tpu_custom_call" | custom-call | tf_op jit(solution)/shard_map/attend/pallas_call | solution.py:322
  42.5 3.6 %all-to-all-start.1 = ((bf16[8,16,1152]{2,1,0:T(8,128)(2,1)}), bf16[8,16,1152]{2,1,0:T(8,128)(2,1)S(1)}, u32[]{:S(2)}, u32[]{:S(2)}) async-start(bf16[8,16,1152]{2,1,0:T(8,128)(2,1)} %get-tuple-element.15), calls=%async_computation.1 | async-start | bytes 589824 | tf_op jit(solution)/shard_map/all_to_all | solution.py:21
  46.1 0.8 dynamic_slice.9
  46.9 9.0 %all-to-all-done.1.parts_ref = bf16[8,16,1152]{2,1,0:T(8,128)(2,1)S(1)} async-done(((bf16[8,16,1152]{2,1,0:T(8,128)(2,1)}), bf16[8,16,1152]{2,1,0:T(8,128)(2,1)S(1)}, u32[]{:S(2)}, u32[]{:S(2)}) %all-to-all-start.1) | async-done | bytes 294944 | tf_op jit(solution)/shard_map/all_to_all | solution.py:21
  55.9 0.0 copy-done
  55.9 0.9 combine.1
  56.8 5.2 %all-gather = bf16[64,512]{1,0:T(8,128)(2,1)S(1)} all-gather(bf16[16,512]{1,0:T(8,128)(2,1)S(1)} %combine.1), channel_id=2, replica_groups=mesh['kv'=8,'tp'=4] {'tp'}, dimensions={0}, use_global_device_ids=true | all-gather | bytes 81920 | tf_op jit(solution)/shard_map/all_gather | solution.py:358
  62.0 2.6 %up.1 = (bf16[8,16,640]{2,1,0:T(8,128)(2,1)S(1)}, bf16[16,512]{1,0:T(8,128)(2,1)S(1)}) custom-call(bf16[16,512]{1,0:T(8,128)(2,1)S(1)} %all_gather.15.block_ref.tokens_ref, bf16[4,16,512]{2,1,0:T(8,128)(2,1)S(1)} %bitcast.6, bf16[1,512]{1,0:T(2,128)(2,1)S(1)} %broadcast_in_dim.18.gain_ref, bf16[512,4096]{1,0:T(8,128)(2,1)} %w_ref.4), custom_call_target="tpu_custom_call" | custom-call | tf_op jit(solution)/shard_map/up/pallas_call | solution.py:365
  64.7 11.4 %all_to_all.20 = bf16[8,16,640]{2,1,0:T(8,128)(2,1)S(1)} all-to-all(bf16[8,16,640]{2,1,0:T(8,128)(2,1)S(1)} %get-tuple-element.18), channel_id=1, replica_groups=mesh['kv'=8,'tp'=4] {'kv'}, dimensions={0} | all-to-all | bytes 327680 | tf_op jit(solution)/shard_map/all_to_all | solution.py:21
  76.1 0.1 slice_reduce_fusion
  76.2 0.1 fusion.2
  76.3 0.7 broadcast_in_dim.19
  77.0 3.4 %all-to-all-start.3 = ((bf16[8,16,512]{2,1,0:T(8,128)(2,1)}), bf16[8,16,512]{2,1,0:T(8,128)(2,1)S(1)}, u32[]{:S(2)}, u32[]{:S(2)}) async-start(bf16[8,16,512]{2,1,0:T(8,128)(2,1)} %broadcast_in_dim.19), calls=%async_computation.3 | async-start | bytes 262144 | tf_op jit(solution)/shard_map/all_to_all | solution.py:21
  80.3 7.3 %all-to-all-done.3.hidden_ref = bf16[8,16,512]{2,1,0:T(8,128)(2,1)S(1)} async-done(((bf16[8,16,512]{2,1,0:T(8,128)(2,1)}), bf16[8,16,512]{2,1,0:T(8,128)(2,1)S(1)}, u32[]{:S(2)}, u32[]{:S(2)}) %all-to-all-start.3) | async-done | bytes 131104 | tf_op jit(solution)/shard_map/all_to_all | solution.py:21
  87.6 2.4 %down.1 = f32[16,512]{1,0:T(8,128)S(1)} custom-call(bf16[8,16,512]{2,1,0:T(8,128)(2,1)S(1)} %all-to-all-done.3.hidden_ref, bf16[4096,512]{1,0:T(8,128)(2,1)} %w_ref.5), custom_call_target="tpu_custom_call" | custom-call | tf_op jit(solution)/shard_map/down/pallas_call | solution.py:385
  90.0 5.4 %all-gather.1 = f32[64,512]{1,0:T(8,128)S(1)} all-gather(f32[16,512]{1,0:T(8,128)S(1)} %down.1), channel_id=3, replica_groups=mesh['kv'=8,'tp'=4] {'tp'}, dimensions={0}, use_global_device_ids=true | all-gather | bytes 163840 | tf_op jit(solution)/shard_map/all_gather | solution.py:396
  95.4 0.6 add_convert_fusion
  (4 shorter events, 0.0 us)
Async XLA Ops:
  10.0 17.1 %all-to-all-start = ((f32[8,16,640]{2,1,0:T(8,128)}), f32[8,16,640]{2,1,0:T(8,128)S(1)}, u32[]{:S(2)}, u32[]{:S(2)}) async-start(f32[8,16,640]{2,1,0:T(8,128)} %get-tuple-element.12), calls=%async_computation | async-start | bytes 655360 | tf_op jit(solution)/shard_map/all_to_all | solution.py:21
  27.1 28.8 %copy-start = (bf16[512,512]{1,0:T(8,128)(2,1)S(1)}, bf16[512,512]{1,0:T(8,128)(2,1)}, u32[]{:S(2)}) copy-start(bf16[512,512]{1,0:T(8,128)(2,1)} %w_ref.3) | copy-start | bytes 1572868
  42.5 13.4 %all-to-all-start.1 = ((bf16[8,16,1152]{2,1,0:T(8,128)(2,1)}), bf16[8,16,1152]{2,1,0:T(8,128)(2,1)S(1)}, u32[]{:S(2)}, u32[]{:S(2)}) async-start(bf16[8,16,1152]{2,1,0:T(8,128)(2,1)} %get-tuple-element.15), calls=%async_computation.1 | async-start | bytes 589824 | tf_op jit(solution)/shard_map/all_to_all | solution.py:21
  77.0 10.7 %all-to-all-start.3 = ((bf16[8,16,512]{2,1,0:T(8,128)(2,1)}), bf16[8,16,512]{2,1,0:T(8,128)(2,1)S(1)}, u32[]{:S(2)}, u32[]{:S(2)}) async-start(bf16[8,16,512]{2,1,0:T(8,128)(2,1)} %broadcast_in_dim.19), calls=%async_computation.3 | async-start | bytes 262144 | tf_op jit(solution)/shard_map/all_to_all | solution.py:21
